TPU v7x, 256 devices: a whole 4x4x8 slice. The times are simulated.
256 devices in a mesh: sp: 64 (over z, x, core), tp: 4 (over y).
Axes of the slice: x: 4, y: 4, z: 8, core: 2. Of those that a mesh axis runs over, the one named last changes fastest.
Arguments:
- residual: bfloat16 [24576, 2048], P(('sp', 'tp')), may hold values from -6 to 6
- queries: bfloat16 [24576, 1024], P('sp', 'tp'), may hold values from -2.5 to 2.5
- keys: bfloat16 [24576, 256], P('sp', 'tp'), may hold values from -2.5 to 2.5
- values: bfloat16 [24576, 256], P('sp', 'tp'), may hold values from -6 to 6
- documents: int32 [24576], P('sp'), may hold values from 0 to 32, never falling along the last dimension, each value on 1 to 1536 neighbouring positions
- sink: float32 [16], P('tp'), may hold values from 3 to 7
- out_weight: bfloat16 [1024, 2048], replicated, may hold values from -0.1875 to 0.1875
- mix_gain: float32 [2048], replicated, may hold values from 0.1 to 1.9
- ffn_gain: float32 [2048], replicated, may hold values from 0.1 to 1.9
- out_gain: float32 [2048], replicated, may hold values from 0.1 to 1.9
- routes: int32 [24576, 4], P(('sp', 'tp')), may hold values from 0 to 63, all different within a row; in each aligned block of 96 rows (0 to 95, 96 to 191, ...) at most 8 rows name the same one
- route_logits: float32 [24576, 4], P(('sp', 'tp')), may hold values from -4 to 4
- gate_weight: bfloat16 [64, 2048, 2048], P('sp', None, 'tp'), may hold values from -1.41421356 to 1.41421356
- up_weight: bfloat16 [64, 2048, 2048], P('sp', None, 'tp'), may hold values from -1.41421356 to 1.41421356
- down_weight: bfloat16 [64, 2048, 2048], P('sp', 'tp'), may hold values from -0.125 to 0.125
Outputs:
- mixed: bfloat16 [24576, 2048], P(('sp', 'tp'))
Inputs may be any that keep to these rules, and one draw needn't show every extreme that they name: `routes`: each row names 4 different experts. In each aligned block of rows held by one device, no expert is named by more than 8 rows, a bound that some block reaches. `documents`: document numbers never fall along the positions; each document has 1 to 1536 positions, and one has exactly 1536.
All inputs are finite; a program needn't handle non-finite values.
Results may differ from a plain program's by a relative error of at most 0.017.
Values may be sent and summed in bfloat16 or wider, within the bound.
A program may use at most 128 MiB of HBM per device.

v0:
```python
import jax
import jax.numpy as jnp
from jax import lax
from jax.sharding import PartitionSpec as P

HD = 64
TOPK = 4
W = 128


def extended(block, sides, width):
    for axis, dim in sides:
        count = lax.axis_size(axis)
        forward = [(i, i + 1) for i in range(count - 1)]
        backward = [(target, source) for source, target in forward]
        low = lax.ppermute(
            lax.slice_in_dim(block, block.shape[dim] - width, None, axis=dim), axis, forward
        )
        high = lax.ppermute(lax.slice_in_dim(block, 0, width, axis=dim), axis, backward)
        block = jnp.concatenate([low, block, high], axis=dim)
    return block


def turn_heads(block, positions, head_count):
    total = block.shape[0]
    heads = block.astype(jnp.float32).reshape(total, head_count, HD)
    half_size = HD // 2
    inverse = 10000.0 ** (-jnp.arange(half_size, dtype=jnp.float32) / half_size)
    angles = positions.astype(jnp.float32)[:, None] * inverse[None, :]
    cosine = jnp.cos(angles)[:, None, :]
    sine = jnp.sin(angles)[:, None, :]
    first_half = heads[..., :half_size]
    second_half = heads[..., half_size:]
    turned = jnp.concatenate(
        [first_half * cosine - second_half * sine, second_half * cosine + first_half * sine],
        axis=-1,
    )
    return turned.reshape(total, head_count * HD).astype(jnp.bfloat16)


def rms_scale(vector):
    return vector * lax.rsqrt(jnp.mean(vector * vector, axis=-1, keepdims=True) + 1e-06)


def windows(padded_rows, blocks):
    tiled = padded_rows.reshape((blocks + 2, W) + padded_rows.shape[1:])
    return jnp.concatenate([tiled[:-2], tiled[1:-1], tiled[2:]], axis=1)


def assign_slots(route_rows, expert_count, capacity):
    flat_routes = route_rows.reshape(route_rows.shape[0] * TOPK)
    onehot_hits = (
        flat_routes[:, None] == jnp.arange(expert_count, dtype=jnp.int32)[None, :]
    ).astype(jnp.int32)
    slot_number = jnp.sum(jnp.cumsum(onehot_hits, axis=0) * onehot_hits, axis=1) - 1
    return flat_routes * capacity + slot_number


def body(
    residual,
    queries,
    keys,
    values,
    documents,
    sink,
    out_weight,
    mix_gain,
    ffn_gain,
    out_gain,
    routes,
    route_logits,
    gate_weight,
    up_weight,
    down_weight,
):
    tok_rows = queries.shape[0]
    head_count = queries.shape[1] // HD
    kv_count = keys.shape[1] // HD
    group_size = head_count // kv_count
    sp_count = lax.axis_size("sp")
    tp_count = lax.axis_size("tp")
    offset = lax.axis_index("sp") * tok_rows
    positions = offset + jnp.arange(tok_rows, dtype=jnp.int32)
    q_turned = turn_heads(queries, positions, head_count)
    k_turned = turn_heads(keys, positions, kv_count)
    paired = jnp.concatenate([k_turned, values], axis=1)
    wide_pairs, wide_docs = (
        extended(paired, (("sp", 0),), W),
        extended(documents, (("sp", 0),), W),
    )
    blocks = tok_rows // W
    query_blocks = q_turned.reshape(blocks, W, kv_count, group_size, HD)
    pair_win = windows(wide_pairs, blocks)
    key_win = pair_win[..., : kv_count * HD].reshape(blocks, 3 * W, kv_count, HD)
    value_win = pair_win[..., kv_count * HD :].reshape(blocks, 3 * W, kv_count, HD)
    doc_win = windows(wide_docs, blocks)
    doc_query = documents.reshape(blocks, W)
    block_ids = jnp.arange(blocks, dtype=jnp.int32)[:, None, None]
    query_pos = offset + block_ids * W + jnp.arange(W, dtype=jnp.int32)[None, :, None]
    key_pos = offset + (block_ids - 1) * W + jnp.arange(3 * W, dtype=jnp.int32)[None, None, :]
    keep_mask = (
        (jnp.abs(query_pos - key_pos) <= W) & (key_pos >= 0) & (key_pos < tok_rows * sp_count)
    )
    keep_mask = keep_mask & (doc_query[:, :, None] == doc_win[:, None, :])
    scores = jnp.einsum(
        "nqhgd,nkhd->nhgqk", query_blocks, key_win, preferred_element_type=jnp.float32
    ) * HD ** (-0.5)
    exponent = jnp.where(keep_mask[:, None, None], jnp.exp(scores), 0.0)
    denominator = jnp.sum(exponent, axis=-1, keepdims=True) + jnp.exp(sink).reshape(
        1, kv_count, group_size, 1, 1
    )
    probs = (exponent / denominator).astype(jnp.bfloat16)
    attended = jnp.einsum("nhgqk,nkhd->nqhgd", probs, value_win, preferred_element_type=jnp.float32)
    attended = attended.astype(jnp.bfloat16).reshape(tok_rows, head_count * HD)
    own_rows = tok_rows // tp_count
    all_heads = lax.all_to_all(attended, "tp", split_axis=0, concat_axis=1, tiled=True)
    projected = jnp.dot(all_heads, out_weight, preferred_element_type=jnp.float32)
    after_mix = residual.astype(jnp.float32) + rms_scale(projected) * mix_gain
    normed = (rms_scale(after_mix) * ffn_gain).astype(jnp.bfloat16)
    local_experts = gate_weight.shape[0]
    expert_count = local_experts * sp_count
    capacity = max(2, own_rows * TOPK * 4 // (3 * expert_count))
    slot_index = assign_slots(routes, expert_count, capacity)
    token_of = jnp.arange(own_rows * TOPK, dtype=jnp.int32) // TOPK
    model_width = normed.shape[1]
    filled = jnp.full((expert_count * capacity,), own_rows, jnp.int32).at[slot_index].set(token_of)
    with_zero = jnp.concatenate([normed, jnp.zeros((1, model_width), jnp.bfloat16)], axis=0)
    outgoing = with_zero[filled].reshape(expert_count, capacity, model_width)
    incoming = lax.all_to_all(outgoing, "sp", split_axis=0, concat_axis=1, tiled=True)
    rows_in = lax.all_gather(incoming, "tp", axis=1, tiled=True)
    gate_pre = jnp.einsum("erd,edf->erf", rows_in, gate_weight, preferred_element_type=jnp.float32)
    up_pre = jnp.einsum("erd,edf->erf", rows_in, up_weight, preferred_element_type=jnp.float32)
    gated = jnp.minimum(gate_pre, 7.0)
    upper = jnp.clip(up_pre, -7.0, 7.0)
    hidden = ((upper + 1.0) * gated * jax.nn.sigmoid(1.702 * gated)).astype(jnp.bfloat16)
    terms = jnp.einsum("erf,efd->erd", hidden, down_weight, preferred_element_type=jnp.float32)
    own_terms = lax.psum_scatter(terms.astype(jnp.bfloat16), "tp", scatter_dimension=1, tiled=True)
    returned = lax.all_to_all(own_terms, "sp", split_axis=1, concat_axis=0, tiled=True)
    picked = returned.reshape(expert_count * capacity, model_width)[slot_index]
    picked = picked.reshape(own_rows, TOPK, model_width).astype(jnp.float32)
    exp_logits = jnp.exp(route_logits)
    route_weights = exp_logits / jnp.sum(exp_logits, axis=-1, keepdims=True)
    expert_mix = jnp.einsum("rk,rkd->rd", route_weights, picked)
    return (after_mix + rms_scale(expert_mix) * out_gain).astype(jnp.bfloat16)


def solution(mesh):
    in_specs = (
        P(("sp", "tp"), None),
        P("sp", "tp"),
        P("sp", "tp"),
        P("sp", "tp"),
        P("sp"),
        P("tp"),
        P(),
        P(),
        P(),
        P(),
        P(("sp", "tp"), None),
        P(("sp", "tp"), None),
        P("sp", None, "tp"),
        P("sp", None, "tp"),
        P("sp", "tp", None),
    )
    out_specs = P(("sp", "tp"), None)
    return jax.shard_map(body, mesh=mesh, in_specs=in_specs, out_specs=out_specs, check_vma=False)
```

profile of v0, /device:TPU:2, one launch (start us, length us, event | category | flops | bytes accessed | tf_op | source)
XLA Modules:
  0.0 421.9 jit_solution(6266095568807970665)
XLA Ops:
  6.6 1.0 bitcast_convert_fusion
  7.5 0.3 fusion.44
  7.8 0.7 fusion.47
  8.6 1.9 collective-permute-start
  10.5 3.6 collective-permute-start.1
  14.1 0.8 fusion.63
  14.9 1.9 collective-permute-start.2
  16.8 3.6 collective-permute-start.3
  20.6 0.3 multiply_cosine_fusion
  20.9 0.8 copy.76
  21.9 0.7 broadcast_multiply_fusion
  22.6 1.1 copy.69
  23.8 0.9 reduce-window.6
  24.7 0.2 slice_reduce_fusion
  25.4 2.9 scatter_custom_fusion
  28.4 0.9 fusion.32
  29.5 0.1 copy.66
  29.7 0.1 copy.67
  30.2 0.7 fusion.17
  30.9 0.7 fusion.23
  31.6 0.3 copy.85
  31.9 1.0 reshape.463
  32.8 4.5 %all-to-all-start = ((bf16[4,96,256]{2,1,0:T(8,128)(2,1)}), bf16[4,96,256]{2,1,0:T(8,128)(2,1)S(1)}, u32[]{:S(2)}, u32[]{:S(2)}) async-start(bf16[4,96,256]{2,1,0:T(8,128)(2,1)} %reshape.463), calls=%async_computation | async-start | bytes 393216 | tf_op jit(solution)/shard_map/all_to_all | solution.py:116
  37.3 6.3 %all-to-all-done = bf16[4,96,256]{2,1,0:T(8,128)(2,1)S(1)} async-done(((bf16[4,96,256]{2,1,0:T(8,128)(2,1)}), bf16[4,96,256]{2,1,0:T(8,128)(2,1)S(1)}, u32[]{:S(2)}, u32[]{:S(2)}) %all-to-all-start) | async-done | bytes 196640 | tf_op jit(solution)/shard_map/all_to_all | solution.py:116
  43.7 3.1 multiply_reduce_fusion.1
  46.8 0.3 multiply_reduce_fusion
  47.2 0.3 multiply_convert_fusion.1
  47.5 3.3 gather_fusion
  50.8 67.5 %all_to_all.40 = bf16[64,8,2048]{2,1,0:T(8,128)(2,1)} all-to-all(bf16[64,8,2048]{2,1,0:T(8,128)(2,1)} %bitcast.134), channel_id=1, replica_groups=mesh['sp'=64,'tp'=4] {'sp'}, dimensions={0} | all-to-all | bytes 4194304 | tf_op jit(solution)/shard_map/all_to_all | solution.py:129
  118.4 0.2 reduce-scatter.2.cloned.1.call-start
  118.6 79.9 %all-gather.2.cloned.1.call-done = bf16[1,2048,2048]{2,1,0:T(8,128)(2,1)} async-done(((bf16[1,512,2048]{2,1,0:T(8,128)(2,1)}), bf16[1,2048,2048]{2,1,0:T(8,128)(2,1)}) %all-gather.2.cloned.1.call-update) | async-done | bytes 8388624 | tf_op jit(solution)/shard_map/all_gather | solution.py:130
  198.5 10.4 %fusion = f32[2048,512]{1,0:T(8,128)} fusion(bf16[1,2048,2048]{2,1,0:T(8,128)(2,1)} %all-gather.2.cloned.1.call-done, bf16[1,2048,512]{2,1,0:T(8,128)(2,1)} %param.27), kind=kOutput, calls=%fused_computation.3 | convolution fusion | flops 4294967296 | bytes 14680064 | tf_op jit(solution)/shard_map/erd,edf->erf/dot_general | solution.py:131
  209.0 15.2 %convert_bitcast_fusion = bf16[1,2048,2048]{2,1,0:T(8,128)(2,1)} fusion(bf16[1,512,2048]{2,1,0:T(8,128)(2,1)S(1)} %copy-done, f32[2048,512]{1,0:T(8,128)} %fusion, bf16[1,2048,2048]{2,1,0:T(8,128)(2,1)} %all-gather.2.cloned.1.call-done, bf16[1,2048,512]{2,1,0:T(8,128)(2,1)} %param.28), kind=kOutput, calls=%fused_computation.7 | convolution fusion | flops 8604614656 | bytes 25165824 | tf_op jit(solution)/shard_map/erf,efd->erd/dot_general | solution.py:136
  224.2 84.2 %reduce-scatter.2.cloned.1.call-done = bf16[1,512,2048]{2,1,0:T(8,128)(2,1)} async-done(((bf16[1,2048,2048]{2,1,0:T(8,128)(2,1)}), bf16[1,512,2048]{2,1,0:T(8,128)(2,1)}) %reduce-scatter.2.cloned.1.call-update) | async-done | bytes 2097168 | tf_op jit(solution)/shard_map/reduce_scatter | solution.py:137
  308.4 6.7 %copy.103 = bf16[1,512,2048]{2,0,1:T(2,128)(2,1)} copy(bf16[1,512,2048]{2,1,0:T(8,128)(2,1)} %reduce-scatter.2.cloned.1.call-done) | data formatting | bytes 4194304 | tf_op jit(solution)/shard_map/reduce_scatter | solution.py:137
  315.1 0.5 broadcast.380
  315.6 13.2 %reduce.5 = bf16[512,2048]{1,0:T(8,128)(2,1)S(1)} reduce(bf16[512,1,2048]{2,1,0:T(2,128)(2,1)} %bitcast.132, bf16[]{:T(256)} %broadcast.380), dimensions={1}, to_apply=%bitcast.129.reduce_sub_computation | reduce | bytes 4194306
  328.8 3.3 reshape.468
  332.1 10.7 %all-to-all-start.2 = ((bf16[64,2,8192]{2,1,0:T(2,128)(2,1)}), bf16[64,2,8192]{2,1,0:T(2,128)(2,1)S(1)}, u32[]{:S(2)}, u32[]{:S(2)}) async-start(bf16[64,2,8192]{2,1,0:T(2,128)(2,1)} %reshape.468), calls=%async_computation.3 | async-start | bytes 4194304 | tf_op jit(solution)/shard_map/all_to_all | solution.py:138
  342.8 0.1 copy.83
  343.0 51.0 %all-to-all-done.2 = bf16[64,2,8192]{2,1,0:T(2,128)(2,1)S(1)} async-done(((bf16[64,2,8192]{2,1,0:T(2,128)(2,1)}), bf16[64,2,8192]{2,1,0:T(2,128)(2,1)S(1)}, u32[]{:S(2)}, u32[]{:S(2)}) %all-to-all-start.2) | async-done | bytes 2097184 | tf_op jit(solution)/shard_map/all_to_all | solution.py:138
  394.0 6.8 %reshape.469 = bf16[512,1,2048]{2,1,0:T(2,128)(2,1)} reshape(bf16[64,2,8192]{2,1,0:T(2,128)(2,1)S(1)} %all-to-all-done.2) | data formatting | bytes 4194304
  400.8 3.5 copy.102
  404.2 3.1 gather_fusion.1
  407.4 3.6 reshape.429
  411.0 2.5 fusion.64
  413.5 0.3 fusion.26
  413.9 1.2 fusion.29
  (69 shorter events, 1.8 us)
Async XLA Ops:
  6.5 202.4 %copy-start = (bf16[1,512,2048]{2,1,0:T(8,128)(2,1)S(1)}, bf16[1,512,2048]{2,1,0:T(8,128)(2,1)}, u32[]{:S(2)}) copy-start(bf16[1,512,2048]{2,1,0:T(8,128)(2,1)} %param.29) | copy-start | bytes 6291460
  6.5 22.7 %copy-start.4 = (bf16[384,64]{0,1:T(8,128)(2,1)S(1)}, bf16[384,64]{0,1:T(8,128)(2,1)}, u32[]{:S(2)}) copy-start(bf16[384,64]{0,1:T(8,128)(2,1)} %param.18) | copy-start | bytes 147460
  6.5 21.8 %copy-start.6 = (s32[384]{0:T(512)S(1)}, s32[384]{0:T(512)}, u32[]{:S(2)}) copy-start(s32[384]{0:T(512)} %param.19) | copy-start | bytes 4612
  6.5 18.8 %copy-start.10 = (f32[4]{0:T(128)S(1)}, f32[4]{0:T(128)}, u32[]{:S(2)}) copy-start(f32[4]{0:T(128)} %param.20) | copy-start | bytes 52
  8.6 20.7 %collective-permute-start = (bf16[128,128]{0,1:T(8,128)(2,1)S(1)}, bf16[128,128]{0,1:T(8,128)(2,1)S(1)}, u32[]{:S(2)}, u32[]{:S(2)}) collective-permute-start(bf16[128,128]{0,1:T(8,128)(2,1)S(1)} %get-tuple-element.12), channel_id=1, source_target_pairs={{0,4},{4,8},{8,12},{12,16},{16,20},{20,24},{24,28},{28,32},{32,36}... | collective-permute-start | bytes 98312 | tf_op jit(solution)/shard_map/ppermute | solution.py:16
  10.5 18.8 %collective-permute-start.1 = (bf16[128,128]{0,1:T(8,128)(2,1)S(1)}, bf16[128,128]{0,1:T(8,128)(2,1)S(1)}, u32[]{:S(2)}, u32[]{:S(2)}) collective-permute-start(bf16[128,128]{0,1:T(8,128)(2,1)S(1)} %get-tuple-element.13), channel_id=1, source_target_pairs={{4,0},{8,4},{12,8},{16,12},{20,16},{24,20},{28,24},{32,28},{36,32}... | collective-permute-start | bytes 98312 | tf_op jit(solution)/shard_map/ppermute | solution.py:19
  14.9 13.4 %collective-permute-start.2 = (s32[128]{0:T(128)S(1)}, s32[128]{0:T(128)S(1)}, u32[]{:S(2)}, u32[]{:S(2)}) collective-permute-start(s32[128]{0:T(128)S(1)} %get-tuple-element.18), channel_id=1, source_target_pairs={{0,4},{4,8},{8,12},{12,16},{16,20},{20,24},{24,28},{28,32},{32,36}... | collective-permute-start | bytes 1544 | tf_op jit(solution)/shard_map/ppermute | solution.py:16
  16.8 11.5 %collective-permute-start.3 = (s32[128]{0:T(128)S(1)}, s32[128]{0:T(128)S(1)}, u32[]{:S(2)}, u32[]{:S(2)}) collective-permute-start(s32[128]{0:T(128)S(1)} %get-tuple-element.19), channel_id=1, source_target_pairs={{4,0},{8,4},{12,8},{16,12},{20,16},{24,20},{28,24},{32,28},{36,32}... | collective-permute-start | bytes 1544 | tf_op jit(solution)/shard_map/ppermute | solution.py:19
  32.8 10.8 %all-to-all-start = ((bf16[4,96,256]{2,1,0:T(8,128)(2,1)}), bf16[4,96,256]{2,1,0:T(8,128)(2,1)S(1)}, u32[]{:S(2)}, u32[]{:S(2)}) async-start(bf16[4,96,256]{2,1,0:T(8,128)(2,1)} %reshape.463), calls=%async_computation | async-start | bytes 393216 | tf_op jit(solution)/shard_map/all_to_all | solution.py:116
  37.3 161.2 %all-gather.2.cloned.1.call-start = ((), (), s32[]{:S(2)}) async-start(), calls=%async_computation.4 | async-start | bytes 10485760 | tf_op jit(solution)/shard_map/all_gather | solution.py:130
  43.6 3.2 copy-start.2
  43.6 3.2 copy-start.5
  43.7 3.5 copy-start.7
  118.4 190.0 %reduce-scatter.2.cloned.1.call-start = ((), (), s32[]{:S(2)}) async-start(), calls=%async_computation.5 | async-start | bytes 10485760 | tf_op jit(solution)/shard_map/reduce_scatter | solution.py:137
  332.1 10.7 %copy-start.9 = (f32[96,4]{0,1:T(4,128)S(1)}, f32[96,4]{0,1:T(4,128)}, u32[]{:S(2)}) copy-start(f32[96,4]{0,1:T(4,128)} %param.26) | copy-start | bytes 4612
  332.1 61.9 %all-to-all-start.2 = ((bf16[64,2,8192]{2,1,0:T(2,128)(2,1)}), bf16[64,2,8192]{2,1,0:T(2,128)(2,1)S(1)}, u32[]{:S(2)}, u32[]{:S(2)}) async-start(bf16[64,2,8192]{2,1,0:T(2,128)(2,1)} %reshape.468), calls=%async_computation.3 | async-start | bytes 4194304 | tf_op jit(solution)/shard_map/all_to_all | solution.py:138
  411.0 2.8 copy-start.3
  411.0 2.8 copy-start.8
  411.0 4.1 copy-start.1
Sparse Core Ops, SparseCore 0:
  118.5 79.9 all-gather.1
  224.3 84.0 reduce-scatter.1
where the time goes:
time: 423 us; the launch traced here: 422 us
  waiting for transfers between devices  221 us (52%)
  blocking collectives  67.5 us (16%)
  local copies, waits for them, and re-layouts  39.3 us (9%)
  matrix products  32.6 us (8%)
  starting transfers between devices  26.5 us (6%)
  other arithmetic  20.7 us (5%)
  between operations  13.8 us (3%)
    reduce_scatter x1, waiting for transfers between devices, body(): lax.psum_scatter(terms.astype(jnp.bfloat16), 'tp', scatter_dimension=1, t...  84.2 us
    all_gather x1, waiting for transfers between devices, body(): rows_in = lax.all_gather(incoming, 'tp', axis=1, tiled=True)  79.9 us
    all_to_all x1, blocking collectives, body(): lax.all_to_all(outgoing, 'sp', split_axis=0, concat_axis=1, tiled=True)  67.5 us
    all_to_all x1, waiting for transfers between devices, body(): lax.all_to_all(own_terms, 'sp', split_axis=1, concat_axis=0, tiled=True)  51 us
    unnamed x28, local copies, waits for them, and re-layouts  15.9 us
    dot_general x1, matrix products, body(): jnp.einsum('erf,efd->erd', hidden, down_weight, preferred_element_type=jn...  15.2 us
    unnamed x1, other arithmetic  13.2 us
    all_to_all x1, starting transfers between devices, body(): lax.all_to_all(own_terms, 'sp', split_axis=1, concat_axis=0, tiled=True)  10.7 us
  transfers between devices with their start and end apart: 8, of which 4 were waited for; matrix products, arithmetic and copies ran while one was open for 2% of the time, Pallas kernels for 0%

commit v1 on v0

--- a/solution.py
+++ b/solution.py
@@ -127,7 +127,9 @@
     with_zero = jnp.concatenate([normed, jnp.zeros((1, model_width), jnp.bfloat16)], axis=0)
     outgoing = with_zero[filled].reshape(expert_count, capacity, model_width)
     incoming = lax.all_to_all(outgoing, "sp", split_axis=0, concat_axis=1, tiled=True)
-    rows_in = lax.all_gather(incoming, "tp", axis=1, tiled=True)
+    rows_in = jnp.concatenate(
+        lax.all_to_all(jnp.stack([incoming] * lax.axis_size("tp")), "tp", 0, 0), axis=1
+    )
     gate_pre = jnp.einsum("erd,edf->erf", rows_in, gate_weight, preferred_element_type=jnp.float32)
     up_pre = jnp.einsum("erd,edf->erf", rows_in, up_weight, preferred_element_type=jnp.float32)
     gated = jnp.minimum(gate_pre, 7.0)

time: 423 us -> 437 us (1.033)
  blocking collectives: 67.5 us -> 163 us
  waiting for transfers between devices: 221 us -> 136 us
  local copies, waits for them, and re-layouts: 39.3 us -> 50.7 us
  matrix products: 32.6 us -> 23.9 us
    all_to_all x0 -> x1, blocking collectives: none -> 95.4 us  [body(): lax.all_to_all(jnp.stack([incoming] * lax.axis_size('tp')), 'tp', 0, 0)]
    all_gather x1 -> x0, waiting for transfers between devices: 79.9 us -> none  [body(): rows_in = lax.all_gather(incoming, 'tp', axis=1, tiled=True)]
    dot_general x1, matrix products: 15.2 us -> 6.79 us  [body(): jnp.einsum('erf,efd->erd', hidden, down_weight, preferred_element_type=jn...]
    unnamed x28 -> x30, local copies, waits for them, and re-layouts: 15.9 us -> 22.5 us
    reduce_scatter x1, waiting for transfers between devices: 84.2 us -> 79 us  [body(): lax.psum_scatter(terms.astype(jnp.bfloat16), 'tp', scatter_dimension=1, t...]
    dot_general x1, matrix products: 10.4 us -> 5.72 us  [body(): jnp.einsum('erd,edf->erf', rows_in, gate_weight, preferred_element_type=j...]
    dot_general x0 -> x1, matrix products: none -> 4.52 us  [body(): jnp.einsum('erd,edf->erf', rows_in, up_weight, preferred_element_type=jnp...]
  transfers between devices with their start and end apart: 8 -> 7, of which waited for: 4 -> 3; matrix products, arithmetic and copies ran while one was open for 2% -> 2% of each run, Pallas kernels for 0% -> 0%
where the time goes in v1:
time: 437 us; the launch traced here: 436 us
  blocking collectives  163 us (37%)
  waiting for transfers between devices  136 us (31%)
  local copies, waits for them, and re-layouts  50.7 us (12%)
  starting transfers between devices  26.4 us (6%)
  matrix products  23.9 us (5%)
  other arithmetic  22.2 us (5%)
  between operations  13.9 us (3%)
    all_to_all x1, blocking collectives, body(): lax.all_to_all(jnp.stack([incoming] * lax.axis_size('tp')), 'tp', 0, 0)  95.4 us
    reduce_scatter x1, waiting for transfers between devices, body(): lax.psum_scatter(terms.astype(jnp.bfloat16), 'tp', scatter_dimension=1, t...  79 us
    all_to_all x1, blocking collectives, body(): lax.all_to_all(outgoing, 'sp', split_axis=0, concat_axis=1, tiled=True)  67.4 us
    all_to_all x1, waiting for transfers between devices, body(): lax.all_to_all(own_terms, 'sp', split_axis=1, concat_axis=0, tiled=True)  51 us
    unnamed x30, local copies, waits for them, and re-layouts  22.5 us
    unnamed x1, other arithmetic  14.7 us
    all_to_all x1, starting transfers between devices, body(): lax.all_to_all(own_terms, 'sp', split_axis=1, concat_axis=0, tiled=True)  10.9 us
  transfers between devices with their start and end apart: 7, of which 3 were waited for; matrix products, arithmetic and copies ran while one was open for 2% of the time, Pallas kernels for 0%

profile of v1, /device:TPU:2, one launch (start us, length us, event | category | flops | bytes accessed | tf_op | source)
XLA Modules:
  0.0 436.3 jit_solution(11198510243865292938)
XLA Ops:
  6.6 1.0 bitcast_convert_fusion
  7.5 0.3 fusion.31
  7.8 0.7 fusion.34
  8.6 1.9 collective-permute-start
  10.5 3.6 collective-permute-start.1
  14.1 0.8 fusion.46
  14.9 1.9 collective-permute-start.2
  16.8 3.6 collective-permute-start.3
  20.6 0.3 multiply_cosine_fusion
  20.9 0.8 copy.76
  21.9 0.7 broadcast_multiply_fusion
  22.6 1.1 copy.69
  23.8 0.9 reduce-window.6
  24.7 0.2 slice_reduce_fusion
  25.4 2.9 scatter_custom_fusion
  28.4 0.9 fusion.19
  29.5 0.1 copy.66
  30.2 0.7 fusion.4
  30.9 0.7 fusion.10
  31.6 0.3 copy.85
  31.9 1.0 reshape.471
  32.8 4.5 %all-to-all-start = ((bf16[4,96,256]{2,1,0:T(8,128)(2,1)}), bf16[4,96,256]{2,1,0:T(8,128)(2,1)S(1)}, u32[]{:S(2)}, u32[]{:S(2)}) async-start(bf16[4,96,256]{2,1,0:T(8,128)(2,1)} %reshape.471), calls=%async_computation | async-start | bytes 393216 | tf_op jit(solution)/shard_map/all_to_all | solution.py:116
  37.3 6.3 %all-to-all-done = bf16[4,96,256]{2,1,0:T(8,128)(2,1)S(1)} async-done(((bf16[4,96,256]{2,1,0:T(8,128)(2,1)}), bf16[4,96,256]{2,1,0:T(8,128)(2,1)S(1)}, u32[]{:S(2)}, u32[]{:S(2)}) %all-to-all-start) | async-done | bytes 196640 | tf_op jit(solution)/shard_map/all_to_all | solution.py:116
  43.7 3.1 multiply_reduce_fusion.1
  46.8 0.3 multiply_reduce_fusion
  47.2 0.3 multiply_convert_fusion.1
  47.5 3.3 gather_fusion
  50.8 67.4 %all_to_all.42 = bf16[64,8,2048]{2,1,0:T(8,128)(2,1)S(1)} all-to-all(bf16[64,8,2048]{2,1,0:T(8,128)(2,1)} %bitcast.127), channel_id=1, replica_groups=mesh['sp'=64,'tp'=4] {'sp'}, dimensions={0} | all-to-all | bytes 4194304 | tf_op jit(solution)/shard_map/all_to_all | solution.py:129
  118.3 1.1 stack.10
  119.4 95.4 %all_to_all.43 = bf16[4,1,512,2048]{3,2,1,0:T(8,128)(2,1)S(1)} all-to-all(bf16[4,1,512,2048]{3,2,1,0:T(8,128)(2,1)S(1)} %stack.10), channel_id=1, replica_groups=mesh['sp'=64,'tp'=4] {'tp'}, dimensions={0} | all-to-all | bytes 16777216 | tf_op jit(solution)/shard_map/all_to_all | solution.py:131
  214.8 4.5 %fusion.2 = f32[2048,512]{1,0:T(8,128)S(1)} fusion(bf16[2048,2048]{1,0:T(8,128)(2,1)S(1)} %bitcast.129, bf16[1,2048,512]{2,1,0:T(8,128)(2,1)S(1)} %copy-done.9), kind=kOutput, calls=%fused_computation.10 | convolution fusion | flops 4294967296 | bytes 14680064 | tf_op jit(solution)/shard_map/erd,edf->erf/dot_general | solution.py:134
  219.3 5.7 %multiply_convert_fusion = bf16[2048,512]{1,0:T(8,128)(2,1)S(1)} fusion(f32[2048,512]{1,0:T(8,128)S(1)} %fusion.2, bf16[2048,2048]{1,0:T(8,128)(2,1)S(1)} %bitcast.130, bf16[1,2048,512]{2,1,0:T(8,128)(2,1)S(1)} %copy-done.10), kind=kOutput, calls=%fused_computation.4 | convolution fusion | flops 4305453056 | bytes 16777216 | tf_op jit(solution)/shard_map/erd,edf->erf/dot_general | solution.py:133
  225.0 6.8 %convert_bitcast_fusion = bf16[1,2048,2048]{2,1,0:T(8,128)(2,1)} fusion(bf16[2048,512]{1,0:T(8,128)(2,1)S(1)} %multiply_convert_fusion, bf16[1,512,2048]{2,1,0:T(8,128)(2,1)S(1)} %copy-done), kind=kOutput, calls=%fused_computation.3 | convolution fusion | flops 4299161600 | bytes 12582912 | tf_op jit(solution)/shard_map/erf,efd->erd/dot_general | solution.py:138
  231.8 79.0 %reduce-scatter.2.cloned.1.call-done = bf16[1,512,2048]{2,1,0:T(8,128)(2,1)} async-done(((bf16[1,2048,2048]{2,1,0:T(8,128)(2,1)}), bf16[1,512,2048]{2,1,0:T(8,128)(2,1)}) %reduce-scatter.2.cloned.1.call-update) | async-done | bytes 2097168 | tf_op jit(solution)/shard_map/reduce_scatter | solution.py:139
  310.8 6.7 %copy.103 = bf16[1,512,2048]{2,0,1:T(2,128)(2,1)} copy(bf16[1,512,2048]{2,1,0:T(8,128)(2,1)} %reduce-scatter.2.cloned.1.call-done) | data formatting | bytes 4194304 | tf_op jit(solution)/shard_map/reduce_scatter | solution.py:139
  317.6 0.5 broadcast.379
  318.1 14.7 %reduce.5 = bf16[512,2048]{1,0:T(8,128)(2,1)} reduce(bf16[512,1,2048]{2,1,0:T(2,128)(2,1)} %bitcast.125, bf16[]{:T(256)} %broadcast.379), dimensions={1}, to_apply=%bitcast.122.reduce_sub_computation | reduce | bytes 4194306
  332.8 4.8 %reshape.476 = bf16[64,2,8192]{2,1,0:T(2,128)(2,1)} reshape(bf16[512,2048]{1,0:T(8,128)(2,1)} %reduce.5) | data formatting | bytes 4194304
  337.6 10.9 %all-to-all-start.3 = ((bf16[64,2,8192]{2,1,0:T(2,128)(2,1)}), bf16[64,2,8192]{2,1,0:T(2,128)(2,1)}, u32[]{:S(2)}, u32[]{:S(2)}) async-start(bf16[64,2,8192]{2,1,0:T(2,128)(2,1)} %reshape.476), calls=%async_computation.4 | async-start | bytes 4194304 | tf_op jit(solution)/shard_map/all_to_all | solution.py:140
  348.5 0.1 copy.83
  348.7 51.0 %all-to-all-done.3 = bf16[64,2,8192]{2,1,0:T(2,128)(2,1)} async-done(((bf16[64,2,8192]{2,1,0:T(2,128)(2,1)}), bf16[64,2,8192]{2,1,0:T(2,128)(2,1)}, u32[]{:S(2)}, u32[]{:S(2)}) %all-to-all-start.3) | async-done | bytes 2097184 | tf_op jit(solution)/shard_map/all_to_all | solution.py:140
  399.6 10.4 %reshape.477 = bf16[512,1,2048]{2,1,0:T(2,128)(2,1)} reshape(bf16[64,2,8192]{2,1,0:T(2,128)(2,1)} %all-to-all-done.3) | data formatting | bytes 4194304
  410.1 4.8 %copy.102 = bf16[1,512,2048]{2,1,0:T(8,128)(2,1)} copy(bf16[1,512,2048]{2,0,1:T(2,128)(2,1)} %bitcast.126) | data formatting | bytes 4194304
  414.9 6.9 %gather_fusion.1 = bf16[384,2048]{1,0:T(8,128)(2,1)} fusion(bf16[512,2048]{1,0:T(8,128)(2,1)} %bitcast.124, s32[1024]{0:T(1024)S(1)} %pad_clamp_fusion), kind=kCustom, calls=%fused_computation.1 | custom fusion | bytes 3147264 | tf_op jit(solution)/shard_map/gather | solution.py:141
  421.8 3.6 reshape.437
  425.5 2.4 fusion.47
  427.9 0.3 fusion.13
  428.2 1.2 fusion.16
  (71 shorter events, 1.9 us)
Async XLA Ops:
  6.5 218.5 %copy-start = (bf16[1,512,2048]{2,1,0:T(8,128)(2,1)S(1)}, bf16[1,512,2048]{2,1,0:T(8,128)(2,1)}, u32[]{:S(2)}) copy-start(bf16[1,512,2048]{2,1,0:T(8,128)(2,1)} %param.29) | copy-start | bytes 6291460
  6.5 22.7 %copy-start.3 = (bf16[384,64]{0,1:T(8,128)(2,1)S(1)}, bf16[384,64]{0,1:T(8,128)(2,1)}, u32[]{:S(2)}) copy-start(bf16[384,64]{0,1:T(8,128)(2,1)} %param.18) | copy-start | bytes 147460
  6.5 21.8 %copy-start.5 = (s32[384]{0:T(512)S(1)}, s32[384]{0:T(512)}, u32[]{:S(2)}) copy-start(s32[384]{0:T(512)} %param.19) | copy-start | bytes 4612
  6.5 18.8 %copy-start.11 = (f32[4]{0:T(128)S(1)}, f32[4]{0:T(128)}, u32[]{:S(2)}) copy-start(f32[4]{0:T(128)} %param.20) | copy-start | bytes 52
  8.6 20.7 %collective-permute-start = (bf16[128,128]{0,1:T(8,128)(2,1)S(1)}, bf16[128,128]{0,1:T(8,128)(2,1)S(1)}, u32[]{:S(2)}, u32[]{:S(2)}) collective-permute-start(bf16[128,128]{0,1:T(8,128)(2,1)S(1)} %get-tuple-element.12), channel_id=1, source_target_pairs={{0,4},{4,8},{8,12},{12,16},{16,20},{20,24},{24,28},{28,32},{32,36}... | collective-permute-start | bytes 98312 | tf_op jit(solution)/shard_map/ppermute | solution.py:16
  10.5 18.8 %collective-permute-start.1 = (bf16[128,128]{0,1:T(8,128)(2,1)S(1)}, bf16[128,128]{0,1:T(8,128)(2,1)S(1)}, u32[]{:S(2)}, u32[]{:S(2)}) collective-permute-start(bf16[128,128]{0,1:T(8,128)(2,1)S(1)} %get-tuple-element.13), channel_id=1, source_target_pairs={{4,0},{8,4},{12,8},{16,12},{20,16},{24,20},{28,24},{32,28},{36,32}... | collective-permute-start | bytes 98312 | tf_op jit(solution)/shard_map/ppermute | solution.py:19
  14.9 13.4 %collective-permute-start.2 = (s32[128]{0:T(128)S(1)}, s32[128]{0:T(128)S(1)}, u32[]{:S(2)}, u32[]{:S(2)}) collective-permute-start(s32[128]{0:T(128)S(1)} %get-tuple-element.18), channel_id=1, source_target_pairs={{0,4},{4,8},{8,12},{12,16},{16,20},{20,24},{24,28},{28,32},{32,36}... | collective-permute-start | bytes 1544 | tf_op jit(solution)/shard_map/ppermute | solution.py:16
  16.8 11.5 %collective-permute-start.3 = (s32[128]{0:T(128)S(1)}, s32[128]{0:T(128)S(1)}, u32[]{:S(2)}, u32[]{:S(2)}) collective-permute-start(s32[128]{0:T(128)S(1)} %get-tuple-element.19), channel_id=1, source_target_pairs={{4,0},{8,4},{12,8},{16,12},{20,16},{24,20},{28,24},{32,28},{36,32}... | collective-permute-start | bytes 1544 | tf_op jit(solution)/shard_map/ppermute | solution.py:19
  32.8 10.8 %all-to-all-start = ((bf16[4,96,256]{2,1,0:T(8,128)(2,1)}), bf16[4,96,256]{2,1,0:T(8,128)(2,1)S(1)}, u32[]{:S(2)}, u32[]{:S(2)}) async-start(bf16[4,96,256]{2,1,0:T(8,128)(2,1)} %reshape.471), calls=%async_computation | async-start | bytes 393216 | tf_op jit(solution)/shard_map/all_to_all | solution.py:116
  37.3 273.5 %reduce-scatter.2.cloned.1.call-start = ((), (), s32[]{:S(2)}) async-start(), calls=%async_computation.5 | async-start | bytes 10485760 | tf_op jit(solution)/shard_map/reduce_scatter | solution.py:139
  43.6 3.2 copy-start.1
  43.6 3.2 copy-start.4
  43.7 3.5 copy-start.6
  119.4 95.4 %copy-start.9 = (bf16[1,2048,512]{2,1,0:T(8,128)(2,1)S(1)}, bf16[1,2048,512]{2,1,0:T(8,128)(2,1)}, u32[]{:S(2)}) copy-start(bf16[1,2048,512]{2,1,0:T(8,128)(2,1)} %param.28) | copy-start | bytes 6291460
  214.8 4.5 %copy-start.10 = (bf16[1,2048,512]{2,1,0:T(8,128)(2,1)S(1)}, bf16[1,2048,512]{2,1,0:T(8,128)(2,1)}, u32[]{:S(2)}) copy-start(bf16[1,2048,512]{2,1,0:T(8,128)(2,1)} %param.27) | copy-start | bytes 6291460
  337.6 10.9 %copy-start.8 = (f32[96,4]{0,1:T(4,128)S(1)}, f32[96,4]{0,1:T(4,128)}, u32[]{:S(2)}) copy-start(f32[96,4]{0,1:T(4,128)} %param.26) | copy-start | bytes 4612
  337.6 62.0 %all-to-all-start.3 = ((bf16[64,2,8192]{2,1,0:T(2,128)(2,1)}), bf16[64,2,8192]{2,1,0:T(2,128)(2,1)}, u32[]{:S(2)}, u32[]{:S(2)}) async-start(bf16[64,2,8192]{2,1,0:T(2,128)(2,1)} %reshape.476), calls=%async_computation.4 | async-start | bytes 4194304 | tf_op jit(solution)/shard_map/all_to_all | solution.py:140
  425.5 2.7 copy-start.2
  425.5 2.7 copy-start.7
Sparse Core Ops, SparseCore 0:
  232.0 78.8 reduce-scatter.1
